TPU v7x, 512 devices: a whole 4x8x8 slice. The times are simulated.
512 devices in a mesh: sp: 32 (over z, x), dp: 16 (over y, core).
Axes of the slice: x: 4, y: 8, z: 8, core: 2. Of those that a mesh axis runs over, the one named last changes fastest.
Arguments:
- query_rows: bfloat16 [16, 4096, 2048], P('dp', 'sp'), may hold values from -6 to 6
- key_rows: bfloat16 [16, 4096, 2048], P('dp', 'sp'), may hold values from -6 to 6
- value_rows: bfloat16 [16, 4096, 2048], P('dp', 'sp'), may hold values from -6 to 6
- decay_low: bfloat16 [16, 4096, 128], P('dp', 'sp'), may hold values from -5 to 5
- rate_low: bfloat16 [16, 4096, 128], P('dp', 'sp'), may hold values from -4 to 4
- decay_up: bfloat16 [128, 2048], replicated, may hold values from -0.5 to 0.5
- rate_up: bfloat16 [128, 2048], replicated, may hold values from -0.5 to 0.5
- decay_base: float32 [2048], replicated, may hold values from -12 to -2
- norm_gain: float32 [2048], replicated, may hold values from 0.1 to 1.9
- out_weight: bfloat16 [2048, 2048], P(None, 'dp'), may hold values from -0.125 to 0.125
Outputs:
- layer_out: bfloat16 [16, 4096, 2048], P('dp', 'sp')
All inputs are finite; a program needn't handle non-finite values.
Results may differ from a plain program's by a relative error of at most 0.005.
Values may be sent and summed in bfloat16 or wider, within the bound.
No kernel may reach another device: no remote copies, remote signals or barrier semaphores. Data moves between devices by JAX's collectives and lax.ppermute only.
A program may use at most 128 MiB of HBM per device.

v0:
```python
import math
import jax
import jax.numpy as jnp
from jax import lax
from jax.sharding import Mesh
from jax.sharding import PartitionSpec as P

HEAD = 64
DP = ("dp_0", "dp_1")
HIGHEST = lax.Precision.HIGHEST
THREE_PASS = lax.Precision.HIGH


def in_order(pieces, dim):
    lengths = list(pieces.shape[1:])
    lengths[dim] *= pieces.shape[0]
    return jnp.moveaxis(pieces, 0, dim).reshape(lengths)


def gather_in_order(value, axes, turns):
    pieces = value
    for k in turns:
        pieces = lax.all_gather(pieces, axes[k])
    done = turns[::-1]
    back = [done.index(k) for k in range(len(axes))]
    pieces = pieces.transpose(*back, *range(len(axes), pieces.ndim))
    return pieces.reshape(-1, *value.shape)


def gathered_by_axis(value, axes, turns, dim):
    return in_order(gather_in_order(value, axes, turns), dim)


def product(form, left, right):
    return jnp.einsum(form, left, right, precision=HIGHEST)


def product_three(form, left, right):
    return jnp.einsum(form, left, right, precision=THREE_PASS)


def to_blocks(rows, heads, block_len):
    positions = rows.shape[0]
    return rows.reshape(positions // block_len, block_len, heads, -1).transpose(2, 0, 3, 1)


def compose(earlier, later):
    return (
        product("hbij,hbjk->hbik", later[0], earlier[0]),
        product("hbij,hbjk->hbik", later[0], earlier[1]) + later[1],
    )


def pre_gates(low_decay, low_rate, decay_up, rate_up, decay_base):
    squashed = jnp.tanh(low_decay.astype(jnp.float32)).astype(jnp.bfloat16)
    decay_pre = (
        decay_base + jnp.dot(squashed, decay_up, preferred_element_type=jnp.float32)
    ).astype(jnp.bfloat16)
    rate_pre = jnp.dot(low_rate, rate_up, preferred_element_type=jnp.float32).astype(jnp.bfloat16)
    return (decay_pre, rate_pre)


def run_mixer(reads, keyed, valued, decay_in, rate_in, gain_here):
    positions = reads.shape[0]
    heads = reads.shape[1] // HEAD
    block_len = math.gcd(positions, 128)
    middle = block_len // 2
    query_blocks = to_blocks(reads.astype(jnp.float32), heads, block_len)
    key_blocks = to_blocks(keyed.astype(jnp.float32), heads, block_len)
    value_blocks = to_blocks(valued.astype(jnp.float32), heads, block_len)
    log_decay = -jnp.exp(-jax.nn.softplus(-decay_in.astype(jnp.float32)) - 0.5)
    decay_blocks = to_blocks(log_decay, heads, block_len)
    rate_blocks = to_blocks(jax.nn.sigmoid(rate_in.astype(jnp.float32)), heads, block_len)
    unit_keys = key_blocks * lax.rsqrt(
        1.0 + jnp.sum(key_blocks * key_blocks, axis=2, keepdims=True)
    )
    erase = unit_keys * rate_blocks
    row_index = lax.broadcasted_iota(jnp.int32, (block_len, block_len), 0)
    col_index = lax.broadcasted_iota(jnp.int32, (block_len, block_len), 1)
    upper = (row_index <= col_index).astype(jnp.float32)
    running = product("hbnc,cd->hbnd", decay_blocks, upper)
    before = running - decay_blocks
    centre = running[..., middle : middle + 1]
    final = running[..., block_len - 1 :]
    read_mid = query_blocks * jnp.exp(running - centre)
    erase_from = unit_keys * jnp.exp(before - centre)
    key_to = key_blocks * jnp.exp(centre - running)
    erase_to = erase * jnp.exp(centre - running)
    read_start = query_blocks * jnp.exp(running)
    erase_start = unit_keys * jnp.exp(before)
    key_end = key_blocks * jnp.exp(final - running)
    erase_end = erase * jnp.exp(final - running)
    strict = row_index > col_index
    within = row_index >= col_index
    key_pairs = jnp.where(strict, product_three("hbnt,hbns->hbts", erase_from, key_to), 0.0)
    erase_pairs = jnp.where(strict, product("hbnt,hbns->hbts", erase_from, erase_to), 0.0)
    read_keys = jnp.where(within, product_three("hbnt,hbns->hbts", read_mid, key_to), 0.0)
    read_erase = jnp.where(within, product_three("hbnt,hbns->hbts", read_mid, erase_to), 0.0)
    lower_matrix = jnp.eye(block_len, dtype=jnp.float32) + erase_pairs
    carried = product_three("hbts,hbms->hbtm", key_pairs, value_blocks)
    right_sides = jnp.concatenate([jnp.swapaxes(erase_start, 2, 3), carried], axis=-1)
    solved = jax.scipy.linalg.solve_triangular(
        lower_matrix, right_sides, lower=True, unit_diagonal=True
    )
    start_weights = solved[..., :HEAD]
    local_erase = solved[..., HEAD:]
    transfer = jnp.eye(HEAD, dtype=jnp.float32) * jnp.exp(final) - product_three(
        "hbnt,hbtk->hbnk", erase_end, start_weights
    )
    added = product_three("hbnt,hbmt->hbnm", key_end, value_blocks) - product_three(
        "hbnt,hbtm->hbnm", erase_end, local_erase
    )
    _, ends = lax.associative_scan(compose, (transfer, added), axis=1)
    starts = jnp.concatenate([jnp.zeros_like(ends[:, :1]), ends[:, :-1]], axis=1)
    read_state = jnp.swapaxes(read_start, 2, 3) - product_three(
        "hbts,hbsn->hbtn", read_erase, start_weights
    )
    readout = (
        product_three("hbtn,hbnm->hbtm", read_state, starts)
        + product_three("hbts,hbms->hbtm", read_keys, value_blocks)
        - product_three("hbts,hbsm->hbtm", read_erase, local_erase)
    )
    average = jnp.mean(readout, axis=-1, keepdims=True)
    centred = readout - average
    variance = jnp.mean(centred * centred, axis=-1, keepdims=True)
    normed = centred * lax.rsqrt(variance + 1.0)
    rows_out = normed.transpose(1, 2, 0, 3).reshape(positions, heads * HEAD)
    return (rows_out * gain_here).astype(jnp.bfloat16)


def per_device(
    query_rows,
    key_rows,
    value_rows,
    decay_low,
    rate_low,
    decay_up,
    rate_up,
    decay_base,
    norm_gain,
    out_weight,
):
    whole_weight = gathered_by_axis(out_weight, DP, (0, 1), 1)
    reads = query_rows[0]
    keyed = key_rows[0]
    valued = value_rows[0]
    decay_pre, rate_pre = pre_gates(decay_low[0], rate_low[0], decay_up, rate_up, decay_base)
    got_reads, got_keys, got_values, got_decay, got_rate = (
        lax.all_to_all(reads, "sp", split_axis=1, concat_axis=0, tiled=True),
        lax.all_to_all(keyed, "sp", split_axis=1, concat_axis=0, tiled=True),
        lax.all_to_all(valued, "sp", split_axis=1, concat_axis=0, tiled=True),
        lax.all_to_all(decay_pre, "sp", split_axis=1, concat_axis=0, tiled=True),
        lax.all_to_all(rate_pre, "sp", split_axis=1, concat_axis=0, tiled=True),
    )
    width_here = got_reads.shape[1]
    gain_here = lax.dynamic_slice_in_dim(norm_gain, lax.axis_index("sp") * width_here, width_here)
    mix = run_mixer(got_reads, got_keys, got_values, got_decay, got_rate, gain_here)
    back = lax.all_to_all(mix, "sp", split_axis=0, concat_axis=1, tiled=True)
    layer_out = jnp.dot(back, whole_weight, preferred_element_type=jnp.float32).astype(jnp.bfloat16)
    return layer_out[None]


def solution(mesh):
    split = Mesh(mesh.devices.reshape(mesh.shape["sp"], 8, 2), ("sp", "dp_0", "dp_1"))
    placed = (
        P(DP, "sp", None),
        P(DP, "sp", None),
        P(DP, "sp", None),
        P(DP, "sp", None),
        P(DP, "sp", None),
        P(),
        P(),
        P(),
        P(),
        P(None, DP),
    )
    return jax.shard_map(
        per_device, mesh=split, in_specs=placed, out_specs=P(DP, "sp", None), check_vma=False
    )
```

profile of v0, /device:TPU:2, one launch (start us, length us, event | category | flops | bytes accessed | tf_op | source)
XLA Modules:
  0.0 559.0 jit_solution(18431480282763413623)
XLA Ops:
  6.5 0.7 all-gather.5.cloned.1.call-update
  7.3 0.3 copy-done
  7.6 1.0 fusion
  8.7 1.0 copy.36
  9.7 13.5 %all-to-all-start.1 = ((bf16[128,32,64]{0,2,1:T(8,128)(2,1)}), bf16[128,32,64]{0,2,1:T(8,128)(2,1)S(1)}, u32[]{:S(2)}, u32[]{:S(2)}) async-start(bf16[128,32,64]{0,2,1:T(8,128)(2,1)} %bitcast.5), calls=%async_computation.1 | async-start | bytes 1048576 | tf_op jit(solution)/shard_map/all_to_all | solution.py:152
  23.1 1.0 copy.37
  24.1 15.8 %all-to-all-done.1 = bf16[128,32,64]{0,2,1:T(8,128)(2,1)S(1)} async-done(((bf16[128,32,64]{0,2,1:T(8,128)(2,1)}), bf16[128,32,64]{0,2,1:T(8,128)(2,1)S(1)}, u32[]{:S(2)}, u32[]{:S(2)}) %all-to-all-start.1) | async-done | bytes 524320 | tf_op jit(solution)/shard_map/all_to_all | solution.py:152
  40.0 5.7 %all-to-all-start.2 = ((bf16[128,32,64]{0,2,1:T(8,128)(2,1)}), bf16[128,32,64]{0,2,1:T(8,128)(2,1)S(1)}, u32[]{:S(2)}, u32[]{:S(2)}) async-start(bf16[128,32,64]{0,2,1:T(8,128)(2,1)} %bitcast.18), calls=%async_computation.2 | async-start | bytes 1048576 | tf_op jit(solution)/shard_map/all_to_all | solution.py:150
  45.7 0.3 convolution_convert_fusion.1
  46.0 1.0 copy.38
  47.1 14.6 %all-to-all-done.2 = bf16[128,32,64]{0,2,1:T(8,128)(2,1)S(1)} async-done(((bf16[128,32,64]{0,2,1:T(8,128)(2,1)}), bf16[128,32,64]{0,2,1:T(8,128)(2,1)S(1)}, u32[]{:S(2)}, u32[]{:S(2)}) %all-to-all-start.2) | async-done | bytes 524320 | tf_op jit(solution)/shard_map/all_to_all | solution.py:150
  61.6 5.6 all-to-all-start.3
  67.2 1.0 copy.39
  68.3 1.0 copy.35
  69.3 1.3 dynamic_slice.3
  70.9 1.4 fusion.50
  72.2 10.9 %all-to-all-done.3 = bf16[128,32,64]{0,2,1:T(8,128)(2,1)S(1)} async-done(((bf16[128,32,64]{0,2,1:T(8,128)(2,1)}), bf16[128,32,64]{0,2,1:T(8,128)(2,1)S(1)}, u32[]{:S(2)}, u32[]{:S(2)}) %all-to-all-start.3) | async-done | bytes 524320 | tf_op jit(solution)/shard_map/all_to_all | solution.py:153
  83.2 0.8 copy-done.14
  84.0 6.1 %all-to-all-start.4 = ((bf16[128,32,64]{0,2,1:T(8,128)(2,1)}), bf16[128,32,64]{0,2,1:T(8,128)(2,1)S(1)}, u32[]{:S(2)}, u32[]{:S(2)}) async-start(bf16[128,32,64]{0,2,1:T(8,128)(2,1)} %bitcast.37), calls=%async_computation.4 | async-start | bytes 1048576 | tf_op jit(solution)/shard_map/all_to_all | solution.py:151
  90.1 1.4 exponential_reduce_fusion
  91.5 5.9 %add_bitcast_fusion = f32[32,1,128,128]{3,2,1,0:T(8,128)} fusion(f32[128,128]{1,0:T(8,128)S(1)} %fusion.149, f32[128,128]{1,0:T(8,128)S(1)} %get-tuple-element.11, pred[128,128]{1,0:T(8,128)(4,1)S(1)} %iota_compare_fusion.1, pred[128,128]{1,0:T(8,128)(4,1)S(1)} %get-tuple-element.10, bf16[128,32,64]{0,2,1:T(8,128)(2,1)S(1)} %all-to-all-done.2, ...), kind=kOutput, calls=%fused_computation.15 | convolution fusion | flops 411303936 | bytes 4907008 | tf_op jit(solution)/shard_map/hbnt,hbns->hbts/dot_general | solution.py:35
  97.4 315.8 %custom-call.4 = f32[32,1,128,128]{2,3,1,0:T(8,128)} custom-call(f32[32,1,128,128]{3,2,1,0:T(8,128)} %add_bitcast_fusion), custom_call_target="InvertDiagBlocksLowerTriangular" | custom-call | tf_op jit(solution)/shard_map/jit(_solve_triangular)/vmap()/triangular_solve | solution.py:102
  413.2 4.0 fusion.60
  417.1 9.8 %all-to-all-start = ((bf16[128,32,64]{0,2,1:T(8,128)(2,1)}), bf16[128,32,64]{0,2,1:T(8,128)(2,1)S(1)}, u32[]{:S(2)}, u32[]{:S(2)}) async-start(bf16[128,32,64]{0,2,1:T(8,128)(2,1)} %bitcast), calls=%async_computation | async-start | bytes 1048576 | tf_op jit(solution)/shard_map/all_to_all | solution.py:149
  426.9 11.6 %all-gather.7.cloned.1.call-start = ((), (), s32[]{:S(2)}) async-start(), calls=%async_computation.7 | async-start | bytes 12582912 | tf_op jit(solution)/shard_map/all_gather | solution.py:23
  438.6 4.2 fusion.23
  442.7 2.0 fusion.71
  444.7 1.7 fusion.56
  446.4 4.3 fusion.14
  450.8 1.4 fusion.30
  452.3 1.3 fusion.29
  453.6 0.7 fusion.37
  454.3 0.7 convolution_bitcast_fusion
  454.9 0.4 fusion.39
  455.3 0.4 convolution_bitcast_fusion.3
  455.7 0.3 fusion.41
  457.1 0.6 pad_maximum_fusion.3
  457.7 2.0 pad.34
  459.7 0.6 pad_add_fusion
  460.4 2.1 pad.35
  462.4 1.7 add.150
  464.1 3.5 pad.37
  467.6 1.3 fusion.42
  468.9 0.7 pad_maximum_fusion.2
  469.5 1.6 pad.36
  471.1 1.7 add.152
  472.8 1.4 fusion.40
  474.4 5.1 pad.39
  479.5 1.9 add.154
  481.4 9.2 %pad.87 = f32[1,32,64,64]{3,2,1,0:T(8,128)} pad(f32[1,16,64,64]{3,2,1,0:T(8,128)} %add.154, f32[]{:T(128)} %constant.12.clone.1), padding=0_0_0x1_0_1x0_0_0x0_0_0 | pad | bytes 786436
  490.5 1.9 fusion.38
  492.5 5.9 %pad.53 = f32[1,31,64,64]{3,2,1,0:T(8,128)} pad(f32[1,16,64,64]{3,2,1,0:T(8,128)S(1)} %pad_maximum_fusion, f32[]{:T(128)} %constant.12.clone.1), padding=0_0_0x0_0_1x0_0_0x0_0_0 | pad | bytes 770052 | tf_op jit(solution)/shard_map/slice | solution.py:114
  498.4 2.8 slice_add_fusion
  501.2 2.6 fusion.65
  503.9 2.2 fusion.34
  506.1 1.0 fusion.52
  507.1 2.8 fusion.58
  509.9 1.6 fusion.26
  511.5 2.2 fusion.178
  514.0 1.1 multiply_convert_fusion
  515.0 9.9 %all-to-all-start.5 = ((bf16[32,128,64]{1,2,0:T(8,128)(2,1)}), bf16[32,128,64]{1,2,0:T(8,128)(2,1)S(1)}, u32[]{:S(2)}, u32[]{:S(2)}) async-start(bf16[32,128,64]{1,2,0:T(8,128)(2,1)} %multiply_convert_fusion), calls=%async_computation.5 | async-start | bytes 1048576 | tf_op jit(solution)/shard_map/all_to_all | solution.py:158
  525.0 7.4 %copy.42 = bf16[8,2,2048,128]{3,2,1,0:T(8,128)(2,1)} copy(bf16[8,2,2048,128]{3,2,0,1:T(8,128)(2,1)} %bitcast.422) | data formatting | bytes 16777216 | tf_op jit(solution)/shard_map/transpose | solution.py:26
  532.4 12.4 %copy.43 = bf16[2048,16,128]{0,2,1:T(8,128)(2,1)} copy(bf16[2048,16,128]{2,0,1:T(8,128)(2,1)} %bitcast.421) | data formatting | bytes 16777216 | tf_op jit(solution)/shard_map/transpose | solution.py:17
  544.8 7.2 %fusion.1 = bf16[1,128,2048]{2,1,0:T(8,128)(2,1)} fusion(bf16[128,2048]{0,1:T(8,128)(2,1)S(1)} %bitcast.424, bf16[2048,2048]{0,1:T(8,128)(2,1)} %bitcast.420), kind=kOutput, calls=%fused_computation.5 | convolution fusion | flops 1074003968 | bytes 9437184 | tf_op jit(solution)/shard_map/dot_general | solution.py:159
  (80 shorter events, 1.8 us)
Async XLA Ops:
  6.5 1.0 copy-start
  6.5 16.6 %copy-start.10 = (bf16[1,128,2048]{2,1,0:T(8,128)(2,1)S(1)}, bf16[1,128,2048]{2,1,0:T(8,128)(2,1)}, u32[]{:S(2)}) copy-start(bf16[1,128,2048]{2,1,0:T(8,128)(2,1)} %param.11) | copy-start | bytes 1572868
  6.5 439.9 %all-gather.5.cloned.1.call-start = ((), (), s32[]{:S(2)}) async-start(), calls=%async_computation.6 | async-start | bytes 4718592 | tf_op jit(solution)/shard_map/all_gather | solution.py:23
  8.6 37.0 %copy-start.11 = (bf16[128,2048]{1,0:T(8,128)(2,1)S(1)}, bf16[128,2048]{1,0:T(8,128)(2,1)}, u32[]{:S(2)}) copy-start(bf16[128,2048]{1,0:T(8,128)(2,1)} %param.16) | copy-start | bytes 1572868
  8.6 37.0 %copy-start.22 = (bf16[1,128,128]{2,1,0:T(8,128)(2,1)S(1)}, bf16[1,128,128]{2,1,0:T(8,128)(2,1)}, u32[]{:S(2)}) copy-start(bf16[1,128,128]{2,1,0:T(8,128)(2,1)} %param.14) | copy-start | bytes 98308
  9.7 30.3 %all-to-all-start.1 = ((bf16[128,32,64]{0,2,1:T(8,128)(2,1)}), bf16[128,32,64]{0,2,1:T(8,128)(2,1)S(1)}, u32[]{:S(2)}, u32[]{:S(2)}) async-start(bf16[128,32,64]{0,2,1:T(8,128)(2,1)} %bitcast.5), calls=%async_computation.1 | async-start | bytes 1048576 | tf_op jit(solution)/shard_map/all_to_all | solution.py:152
  40.0 27.3 %copy-start.12 = (bf16[1,128,2048]{2,1,0:T(8,128)(2,1)S(1)}, bf16[1,128,2048]{2,1,0:T(8,128)(2,1)}, u32[]{:S(2)}) copy-start(bf16[1,128,2048]{2,1,0:T(8,128)(2,1)} %param.12) | copy-start | bytes 1572868
  40.0 21.7 %all-to-all-start.2 = ((bf16[128,32,64]{0,2,1:T(8,128)(2,1)}), bf16[128,32,64]{0,2,1:T(8,128)(2,1)S(1)}, u32[]{:S(2)}, u32[]{:S(2)}) async-start(bf16[128,32,64]{0,2,1:T(8,128)(2,1)} %bitcast.18), calls=%async_computation.2 | async-start | bytes 1048576 | tf_op jit(solution)/shard_map/all_to_all | solution.py:150
  45.7 22.6 %copy-start.13 = (bf16[1,128,2048]{2,1,0:T(8,128)(2,1)S(1)}, bf16[1,128,2048]{2,1,0:T(8,128)(2,1)}, u32[]{:S(2)}) copy-start(bf16[1,128,2048]{2,1,0:T(8,128)(2,1)} %param.10) | copy-start | bytes 1572868
  61.6 21.5 %all-to-all-start.3 = ((bf16[128,32,64]{0,2,1:T(8,128)(2,1)}), bf16[128,32,64]{0,2,1:T(8,128)(2,1)S(1)}, u32[]{:S(2)}, u32[]{:S(2)}) async-start(bf16[128,32,64]{0,2,1:T(8,128)(2,1)} %bitcast.25), calls=%async_computation.3 | async-start | bytes 1048576 | tf_op jit(solution)/shard_map/all_to_all | solution.py:153
  70.9 381.4 %copy-start.20 = (f32[32,128]{1,0:T(8,128)}, f32[32,128]{1,0:T(8,128)S(1)}, u32[]{:S(2)}) copy-start(f32[32,128]{1,0:T(8,128)S(1)} %add_rsqrt_fusion.1) | copy-start | bytes 49156
  83.2 0.8 copy-start.14
  84.0 333.2 %all-to-all-start.4 = ((bf16[128,32,64]{0,2,1:T(8,128)(2,1)}), bf16[128,32,64]{0,2,1:T(8,128)(2,1)S(1)}, u32[]{:S(2)}, u32[]{:S(2)}) async-start(bf16[128,32,64]{0,2,1:T(8,128)(2,1)} %bitcast.37), calls=%async_computation.4 | async-start | bytes 1048576 | tf_op jit(solution)/shard_map/all_to_all | solution.py:151
  90.1 1.5 copy-start.15
  91.5 321.7 %copy-start.18 = (f32[32,64]{1,0:T(8,128)}, f32[32,64]{1,0:T(8,128)S(1)}, u32[]{:S(2)}) copy-start(f32[32,64]{1,0:T(8,128)S(1)} %get-tuple-element.7) | copy-start | bytes 24580
  417.1 84.0 %all-to-all-start = ((bf16[128,32,64]{0,2,1:T(8,128)(2,1)}), bf16[128,32,64]{0,2,1:T(8,128)(2,1)S(1)}, u32[]{:S(2)}, u32[]{:S(2)}) async-start(bf16[128,32,64]{0,2,1:T(8,128)(2,1)} %bitcast), calls=%async_computation | async-start | bytes 1048576 | tf_op jit(solution)/shard_map/all_to_all | solution.py:149
  426.9 98.0 %all-gather.7.cloned.1.call-start = ((), (), s32[]{:S(2)}) async-start(), calls=%async_computation.7 | async-start | bytes 12582912 | tf_op jit(solution)/shard_map/all_gather | solution.py:23
  446.4 4.4 copy-start.8
  446.4 4.4 copy-start.16
  450.8 1.5 copy-start.2
  452.3 1.3 copy-start.7
  453.6 2.1 copy-start.4
  454.3 2.2 copy-start.6
  455.3 1.2 copy-start.9
  456.7 12.1 %slice-start.2 = ((f32[1,8,64,64]{3,2,1,0:T(8,128)}), f32[1,1,64,64]{3,2,1,0:T(8,128)S(1)}, s32[]{:S(2)}) async-start(f32[1,8,64,64]{3,2,1,0:T(8,128)} %copy-done.9), calls=%async_computation.10 | async-start | bytes 65536 | tf_op jit(solution)/shard_map/slice | solution.py:113
  459.7 14.5 %slice-start = ((f32[1,16,64,64]{3,2,1,0:T(8,128)}), f32[1,1,64,64]{3,2,1,0:T(8,128)S(1)}, s32[]{:S(2)}) async-start(f32[1,16,64,64]{3,2,1,0:T(8,128)} %copy-done.6), calls=%async_computation.8 | async-start | bytes 65536 | tf_op jit(solution)/shard_map/slice | solution.py:113
  481.4 11.1 %slice-start.1 = ((f32[1,32,64,64]{3,2,1,0:T(8,128)}), f32[1,1,64,64]{3,2,1,0:T(8,128)S(1)}, s32[]{:S(2)}) async-start(f32[1,32,64,64]{3,2,1,0:T(8,128)} %copy-done.7), calls=%async_computation.9 | async-start | bytes 65536 | tf_op jit(solution)/shard_map/slice | solution.py:113
  492.5 8.7 %copy-start.19 = (f32[32,64]{1,0:T(8,128)S(1)}, f32[32,64]{1,0:T(8,128)}, u32[]{:S(2)}) copy-start(f32[32,64]{1,0:T(8,128)} %copy-done.18) | copy-start | bytes 24580
  492.5 8.6 %copy-start.21 = (f32[32,128]{1,0:T(8,128)S(1)}, f32[32,128]{1,0:T(8,128)}, u32[]{:S(2)}) copy-start(f32[32,128]{1,0:T(8,128)} %copy-done.20) | copy-start | bytes 49156
  498.4 2.8 copy-start.17
  501.2 2.7 copy-start.3
  503.9 2.3 copy-start.5
  511.5 2.4 copy-start.23
  515.0 29.7 %all-to-all-start.5 = ((bf16[32,128,64]{1,2,0:T(8,128)(2,1)}), bf16[32,128,64]{1,2,0:T(8,128)(2,1)S(1)}, u32[]{:S(2)}, u32[]{:S(2)}) async-start(bf16[32,128,64]{1,2,0:T(8,128)(2,1)} %multiply_convert_fusion), calls=%async_computation.5 | async-start | bytes 1048576 | tf_op jit(solution)/shard_map/all_to_all | solution.py:158
  544.8 7.2 %copy-start.1 = (bf16[128,2048]{1,0:T(8,128)(2,1)S(1)}, bf16[128,2048]{1,0:T(8,128)(2,1)}, u32[]{:S(2)}) copy-start(bf16[128,2048]{1,0:T(8,128)(2,1)} %param.15) | copy-start | bytes 1572868
Sparse Core Ops, SparseCore 0:
  9.4 61.7 all-gather.4
  446.5 28.9 all-gather.6
where the time goes:
time: 566 us; the launch traced here: 559 us
  other arithmetic  329 us (58%)
  starting transfers between devices  62.1 us (11%)
  local copies, waits for them, and re-layouts  58.2 us (10%)
  matrix products  53 us (9%)
  waiting for transfers between devices  42.1 us (7%)
  between operations  14.3 us (3%)
    another operation x4, other arithmetic, run_mixer(): jax.scipy.linalg.solve_triangular(lower_matrix, right_sides, lower=True,...  316 us
    dot_general x11, matrix products, product_three(): return jnp.einsum(form, left, right, precision=THREE_PASS)  25 us
    all_to_all x1, waiting for transfers between devices, per_device(): lax.all_to_all(decay_pre, 'sp', split_axis=1, concat_axis=0, tiled=True)  15.8 us
    dot_general x15, matrix products, product(): return jnp.einsum(form, left, right, precision=HIGHEST)  15.2 us
    all_to_all x1, waiting for transfers between devices, per_device(): lax.all_to_all(keyed, 'sp', split_axis=1, concat_axis=0, tiled=True)  14.6 us
    pad x6, local copies, waits for them, and re-layouts, run_mixer(): _, ends = lax.associative_scan(compose, (transfer, added), axis=1)  14.3 us
    all_to_all x1, starting transfers between devices, per_device(): lax.all_to_all(decay_pre, 'sp', split_axis=1, concat_axis=0, tiled=True)  13.5 us
    unnamed x52, local copies, waits for them, and re-layouts  13.4 us
  transfers between devices with their start and end apart: 8, of which 3 were waited for; matrix products, arithmetic and copies ran while one was open for 77% of the time, Pallas kernels for 0%

commit v1 on v0

--- a/solution.py
+++ b/solution.py
@@ -9,6 +9,12 @@
 DP = ("dp_0", "dp_1")
 HIGHEST = lax.Precision.HIGHEST
 THREE_PASS = lax.Precision.HIGH
+
+
+def stacked_exchange(x, mesh_axis, split, join):
+    pieces = jnp.split(x, lax.axis_size(mesh_axis), axis=split)
+    incoming = lax.all_to_all(jnp.stack(pieces), mesh_axis, 0, 0)
+    return jnp.concatenate(incoming, axis=join)
 
 
 def in_order(pieces, dim):
@@ -149,7 +155,7 @@
         lax.all_to_all(reads, "sp", split_axis=1, concat_axis=0, tiled=True),
         lax.all_to_all(keyed, "sp", split_axis=1, concat_axis=0, tiled=True),
         lax.all_to_all(valued, "sp", split_axis=1, concat_axis=0, tiled=True),
-        lax.all_to_all(decay_pre, "sp", split_axis=1, concat_axis=0, tiled=True),
+        stacked_exchange(decay_pre, "sp", 1, 0),
         lax.all_to_all(rate_pre, "sp", split_axis=1, concat_axis=0, tiled=True),
     )
     width_here = got_reads.shape[1]

time: 566 us -> 558 us (0.986)
  the two profiles are of different devices: /device:TPU:2 before, /device:TPU:26 now
where the time goes in v1:
time: 558 us; the launch traced here: 550 us
  other arithmetic  329 us (59%)
  local copies, waits for them, and re-layouts  60.2 us (11%)
  matrix products  53.2 us (10%)
  starting transfers between devices  50.6 us (9%)
  waiting for transfers between devices  42.1 us (8%)
  between operations  14.5 us (3%)
    another operation x4, other arithmetic, run_mixer(): jax.scipy.linalg.solve_triangular(lower_matrix, right_sides, lower=True,...  316 us
    dot_general x11, matrix products, product_three(): return jnp.einsum(form, left, right, precision=THREE_PASS)  25.2 us
    all_to_all x1, waiting for transfers between devices, stacked_exchange(): incoming = lax.all_to_all(jnp.stack(pieces), mesh_axis, 0, 0)  15.8 us
    dot_general x15, matrix products, product(): return jnp.einsum(form, left, right, precision=HIGHEST)  15.2 us
    unnamed x83, local copies, waits for them, and re-layouts  15.1 us
    all_to_all x1, waiting for transfers between devices, per_device(): lax.all_to_all(keyed, 'sp', split_axis=1, concat_axis=0, tiled=True)  14.6 us
    pad x6, local copies, waits for them, and re-layouts, run_mixer(): _, ends = lax.associative_scan(compose, (transfer, added), axis=1)  14.3 us
    all_to_all x1, starting transfers between devices, stacked_exchange(): incoming = lax.all_to_all(jnp.stack(pieces), mesh_axis, 0, 0)  13.5 us
  transfers between devices with their start and end apart: 8, of which 3 were waited for; matrix products, arithmetic and copies ran while one was open for 79% of the time, Pallas kernels for 0%

profile of v1, /device:TPU:26, one launch (start us, length us, event | category | flops | bytes accessed | tf_op | source)
XLA Modules:
  0.0 549.8 jit_solution(1613645323860984914)
XLA Ops:
  6.5 0.7 all-gather.5.cloned.1.call-update
  7.3 0.3 copy-done
  7.6 1.0 fusion
  10.6 1.1 copy.100
  11.7 13.5 %all-to-all-start.1 = ((bf16[32,128,64]{1,2,0:T(8,128)(2,1)}), bf16[32,128,64]{1,2,0:T(8,128)(2,1)S(1)}, u32[]{:S(2)}, u32[]{:S(2)}) async-start(bf16[32,128,64]{1,2,0:T(8,128)(2,1)} %copy.100), calls=%async_computation.1 | async-start | bytes 1048576 | tf_op jit(solution)/shard_map/all_to_all | solution.py:16
  25.2 1.0 copy.101
  26.2 15.8 %all-to-all-done.1 = bf16[32,128,64]{1,2,0:T(8,128)(2,1)S(1)} async-done(((bf16[32,128,64]{1,2,0:T(8,128)(2,1)}), bf16[32,128,64]{1,2,0:T(8,128)(2,1)S(1)}, u32[]{:S(2)}, u32[]{:S(2)}) %all-to-all-start.1) | async-done | bytes 524320 | tf_op jit(solution)/shard_map/all_to_all | solution.py:16
  42.0 5.7 %all-to-all-start.2 = ((bf16[128,32,64]{0,2,1:T(8,128)(2,1)}), bf16[128,32,64]{0,2,1:T(8,128)(2,1)S(1)}, u32[]{:S(2)}, u32[]{:S(2)}) async-start(bf16[128,32,64]{0,2,1:T(8,128)(2,1)} %bitcast.48), calls=%async_computation.2 | async-start | bytes 1048576 | tf_op jit(solution)/shard_map/all_to_all | solution.py:156
  47.8 0.3 convolution_convert_fusion.1
  48.1 1.0 copy.102
  49.2 14.6 %all-to-all-done.2 = bf16[128,32,64]{0,2,1:T(8,128)(2,1)S(1)} async-done(((bf16[128,32,64]{0,2,1:T(8,128)(2,1)}), bf16[128,32,64]{0,2,1:T(8,128)(2,1)S(1)}, u32[]{:S(2)}, u32[]{:S(2)}) %all-to-all-start.2) | async-done | bytes 524320 | tf_op jit(solution)/shard_map/all_to_all | solution.py:156
  63.7 5.6 %all-to-all-start.3 = ((bf16[128,32,64]{0,2,1:T(8,128)(2,1)}), bf16[128,32,64]{0,2,1:T(8,128)(2,1)S(1)}, u32[]{:S(2)}, u32[]{:S(2)}) async-start(bf16[128,32,64]{0,2,1:T(8,128)(2,1)} %bitcast.55), calls=%async_computation.3 | async-start | bytes 1048576 | tf_op jit(solution)/shard_map/all_to_all | solution.py:159
  69.3 1.0 copy.99
  70.3 1.0 copy.103
  71.3 1.3 dynamic_slice.3
  72.9 1.4 fusion.50
  74.3 10.9 %all-to-all-done.3 = bf16[128,32,64]{0,2,1:T(8,128)(2,1)S(1)} async-done(((bf16[128,32,64]{0,2,1:T(8,128)(2,1)}), bf16[128,32,64]{0,2,1:T(8,128)(2,1)S(1)}, u32[]{:S(2)}, u32[]{:S(2)}) %all-to-all-start.3) | async-done | bytes 524320 | tf_op jit(solution)/shard_map/all_to_all | solution.py:159
  85.3 0.8 copy-done.14
  86.1 6.1 %all-to-all-start.4 = ((bf16[128,32,64]{0,2,1:T(8,128)(2,1)}), bf16[128,32,64]{0,2,1:T(8,128)(2,1)S(1)}, u32[]{:S(2)}, u32[]{:S(2)}) async-start(bf16[128,32,64]{0,2,1:T(8,128)(2,1)} %bitcast.67), calls=%async_computation.4 | async-start | bytes 1048576 | tf_op jit(solution)/shard_map/all_to_all | solution.py:157
  92.2 1.4 exponential_reduce_fusion
  93.7 5.9 %add_bitcast_fusion = f32[32,1,128,128]{3,2,1,0:T(8,128)} fusion(f32[128,128]{1,0:T(8,128)S(1)} %fusion.145, f32[128,128]{1,0:T(8,128)S(1)} %get-tuple-element.11, pred[128,128]{1,0:T(8,128)(4,1)S(1)} %iota_compare_fusion.1, pred[128,128]{1,0:T(8,128)(4,1)S(1)} %get-tuple-element.10, bf16[128,32,64]{0,2,1:T(8,128)(2,1)S(1)} %all-to-all-done.2, ...), kind=kOutput, calls=%fused_computation.15 | convolution fusion | flops 411303936 | bytes 4907008 | tf_op jit(solution)/shard_map/hbnt,hbns->hbts/dot_general | solution.py:41
  99.6 315.8 %custom-call.4 = f32[32,1,128,128]{2,3,1,0:T(8,128)} custom-call(f32[32,1,128,128]{3,2,1,0:T(8,128)} %add_bitcast_fusion), custom_call_target="InvertDiagBlocksLowerTriangular" | custom-call | tf_op jit(solution)/shard_map/jit(_solve_triangular)/vmap()/triangular_solve | solution.py:108
  415.4 4.0 fusion.60
  419.3 9.8 %all-to-all-start = ((bf16[128,32,64]{0,2,1:T(8,128)(2,1)}), bf16[128,32,64]{0,2,1:T(8,128)(2,1)S(1)}, u32[]{:S(2)}, u32[]{:S(2)}) async-start(bf16[128,32,64]{0,2,1:T(8,128)(2,1)} %bitcast), calls=%async_computation | async-start | bytes 1048576 | tf_op jit(solution)/shard_map/all_to_all | solution.py:155
  429.1 4.2 fusion.23
  433.3 2.0 fusion.71
  435.3 1.7 fusion.56
  437.0 4.3 fusion.14
  441.4 1.6 fusion.30
  443.0 1.3 fusion.29
  444.3 0.7 fusion.37
  445.0 0.7 convolution_bitcast_fusion
  445.7 0.4 fusion.39
  446.1 0.4 convolution_bitcast_fusion.3
  446.5 0.3 fusion.41
  446.8 0.3 convolution_bitcast_fusion.6
  447.8 0.6 pad_maximum_fusion.3
  448.4 2.0 pad.34
  450.5 0.6 pad_add_fusion
  451.1 2.1 pad.35
  453.2 1.7 add.150
  454.9 3.5 pad.37
  458.3 1.3 fusion.42
  459.6 0.7 pad_maximum_fusion.2
  460.3 1.6 pad.36
  461.9 1.7 add.152
  463.6 1.4 fusion.40
  465.1 5.1 pad.39
  470.2 1.9 add.154
  472.1 9.2 %pad.87 = f32[1,32,64,64]{3,2,1,0:T(8,128)} pad(f32[1,16,64,64]{3,2,1,0:T(8,128)} %add.154, f32[]{:T(128)} %constant.12.clone.1), padding=0_0_0x1_0_1x0_0_0x0_0_0 | pad | bytes 786436
  481.3 1.9 fusion.38
  483.3 5.9 %pad.53 = f32[1,31,64,64]{3,2,1,0:T(8,128)} pad(f32[1,16,64,64]{3,2,1,0:T(8,128)S(1)} %pad_maximum_fusion, f32[]{:T(128)} %constant.12.clone.1), padding=0_0_0x0_0_1x0_0_0x0_0_0 | pad | bytes 770052 | tf_op jit(solution)/shard_map/slice | solution.py:120
  489.2 2.8 slice_add_fusion
  491.9 2.6 fusion.65
  494.6 2.2 fusion.34
  496.9 1.0 fusion.52
  497.9 2.8 fusion.58
  500.7 1.6 fusion.26
  502.3 2.2 fusion.174
  504.7 1.1 multiply_convert_fusion
  505.8 9.9 %all-to-all-start.5 = ((bf16[32,128,64]{1,2,0:T(8,128)(2,1)}), bf16[32,128,64]{1,2,0:T(8,128)(2,1)S(1)}, u32[]{:S(2)}, u32[]{:S(2)}) async-start(bf16[32,128,64]{1,2,0:T(8,128)(2,1)} %multiply_convert_fusion), calls=%async_computation.5 | async-start | bytes 1048576 | tf_op jit(solution)/shard_map/all_to_all | solution.py:164
  515.7 7.4 %copy.106 = bf16[8,2,2048,128]{3,2,1,0:T(8,128)(2,1)} copy(bf16[8,2,2048,128]{3,2,0,1:T(8,128)(2,1)} %bitcast.520) | data formatting | bytes 16777216 | tf_op jit(solution)/shard_map/transpose | solution.py:32
  523.2 12.4 %copy.107 = bf16[2048,16,128]{0,2,1:T(8,128)(2,1)} copy(bf16[2048,16,128]{2,0,1:T(8,128)(2,1)} %bitcast.519) | data formatting | bytes 16777216 | tf_op jit(solution)/shard_map/transpose | solution.py:23
  535.5 7.2 %fusion.1 = bf16[1,128,2048]{2,1,0:T(8,128)(2,1)} fusion(bf16[128,2048]{0,1:T(8,128)(2,1)S(1)} %bitcast.522, bf16[2048,2048]{0,1:T(8,128)(2,1)} %bitcast.518), kind=kOutput, calls=%fused_computation.5 | convolution fusion | flops 1074003968 | bytes 9437184 | tf_op jit(solution)/shard_map/dot_general | solution.py:165
  (112 shorter events, 3.4 us)
Async XLA Ops:
  6.5 1.0 copy-start
  6.5 430.4 %all-gather.5.cloned.1.call-start = ((), (), s32[]{:S(2)}) async-start(), calls=%async_computation.6 | async-start | bytes 4718592 | tf_op jit(solution)/shard_map/all_gather | solution.py:29
  9.1 16.1 %copy-start.10 = (bf16[1,128,2048]{2,1,0:T(8,128)(2,1)S(1)}, bf16[1,128,2048]{2,1,0:T(8,128)(2,1)}, u32[]{:S(2)}) copy-start(bf16[1,128,2048]{2,1,0:T(8,128)(2,1)} %param.11) | copy-start | bytes 1572868
  10.6 37.2 %copy-start.11 = (bf16[128,2048]{1,0:T(8,128)(2,1)S(1)}, bf16[128,2048]{1,0:T(8,128)(2,1)}, u32[]{:S(2)}) copy-start(bf16[128,2048]{1,0:T(8,128)(2,1)} %param.16) | copy-start | bytes 1572868
  10.6 37.2 %copy-start.22 = (bf16[1,128,128]{2,1,0:T(8,128)(2,1)S(1)}, bf16[1,128,128]{2,1,0:T(8,128)(2,1)}, u32[]{:S(2)}) copy-start(bf16[1,128,128]{2,1,0:T(8,128)(2,1)} %param.14) | copy-start | bytes 98308
  11.7 30.3 %all-to-all-start.1 = ((bf16[32,128,64]{1,2,0:T(8,128)(2,1)}), bf16[32,128,64]{1,2,0:T(8,128)(2,1)S(1)}, u32[]{:S(2)}, u32[]{:S(2)}) async-start(bf16[32,128,64]{1,2,0:T(8,128)(2,1)} %copy.100), calls=%async_computation.1 | async-start | bytes 1048576 | tf_op jit(solution)/shard_map/all_to_all | solution.py:16
  42.0 27.3 %copy-start.12 = (bf16[1,128,2048]{2,1,0:T(8,128)(2,1)S(1)}, bf16[1,128,2048]{2,1,0:T(8,128)(2,1)}, u32[]{:S(2)}) copy-start(bf16[1,128,2048]{2,1,0:T(8,128)(2,1)} %param.10) | copy-start | bytes 1572868
  42.0 21.7 %all-to-all-start.2 = ((bf16[128,32,64]{0,2,1:T(8,128)(2,1)}), bf16[128,32,64]{0,2,1:T(8,128)(2,1)S(1)}, u32[]{:S(2)}, u32[]{:S(2)}) async-start(bf16[128,32,64]{0,2,1:T(8,128)(2,1)} %bitcast.48), calls=%async_computation.2 | async-start | bytes 1048576 | tf_op jit(solution)/shard_map/all_to_all | solution.py:156
  47.8 22.6 %copy-start.13 = (bf16[1,128,2048]{2,1,0:T(8,128)(2,1)S(1)}, bf16[1,128,2048]{2,1,0:T(8,128)(2,1)}, u32[]{:S(2)}) copy-start(bf16[1,128,2048]{2,1,0:T(8,128)(2,1)} %param.12) | copy-start | bytes 1572868
  63.7 21.5 %all-to-all-start.3 = ((bf16[128,32,64]{0,2,1:T(8,128)(2,1)}), bf16[128,32,64]{0,2,1:T(8,128)(2,1)S(1)}, u32[]{:S(2)}, u32[]{:S(2)}) async-start(bf16[128,32,64]{0,2,1:T(8,128)(2,1)} %bitcast.55), calls=%async_computation.3 | async-start | bytes 1048576 | tf_op jit(solution)/shard_map/all_to_all | solution.py:159
  72.9 370.1 %copy-start.20 = (f32[32,128]{1,0:T(8,128)}, f32[32,128]{1,0:T(8,128)S(1)}, u32[]{:S(2)}) copy-start(f32[32,128]{1,0:T(8,128)S(1)} %add_rsqrt_fusion.1) | copy-start | bytes 49156
  85.3 0.8 copy-start.14
  86.1 333.2 %all-to-all-start.4 = ((bf16[128,32,64]{0,2,1:T(8,128)(2,1)}), bf16[128,32,64]{0,2,1:T(8,128)(2,1)S(1)}, u32[]{:S(2)}, u32[]{:S(2)}) async-start(bf16[128,32,64]{0,2,1:T(8,128)(2,1)} %bitcast.67), calls=%async_computation.4 | async-start | bytes 1048576 | tf_op jit(solution)/shard_map/all_to_all | solution.py:157
  92.2 1.5 copy-start.15
  93.7 321.7 %copy-start.18 = (f32[32,64]{1,0:T(8,128)}, f32[32,64]{1,0:T(8,128)S(1)}, u32[]{:S(2)}) copy-start(f32[32,64]{1,0:T(8,128)S(1)} %get-tuple-element.7) | copy-start | bytes 24580
  419.3 72.6 %all-to-all-start = ((bf16[128,32,64]{0,2,1:T(8,128)(2,1)}), bf16[128,32,64]{0,2,1:T(8,128)(2,1)S(1)}, u32[]{:S(2)}, u32[]{:S(2)}) async-start(bf16[128,32,64]{0,2,1:T(8,128)(2,1)} %bitcast), calls=%async_computation | async-start | bytes 1048576 | tf_op jit(solution)/shard_map/all_to_all | solution.py:155
  429.1 86.6 %all-gather.7.cloned.1.call-start = ((), (), s32[]{:S(2)}) async-start(), calls=%async_computation.7 | async-start | bytes 12582912 | tf_op jit(solution)/shard_map/all_gather | solution.py:29
  437.0 4.4 copy-start.8
  437.0 4.4 copy-start.16
  441.4 1.6 copy-start.2
  443.0 1.3 copy-start.7
  444.3 2.1 copy-start.4
  445.0 2.2 copy-start.6
  446.1 1.2 copy-start.9
  447.5 12.1 %slice-start.2 = ((f32[1,8,64,64]{3,2,1,0:T(8,128)}), f32[1,1,64,64]{3,2,1,0:T(8,128)S(1)}, s32[]{:S(2)}) async-start(f32[1,8,64,64]{3,2,1,0:T(8,128)} %copy-done.9), calls=%async_computation.10 | async-start | bytes 65536 | tf_op jit(solution)/shard_map/slice | solution.py:119
  450.5 14.5 %slice-start = ((f32[1,16,64,64]{3,2,1,0:T(8,128)}), f32[1,1,64,64]{3,2,1,0:T(8,128)S(1)}, s32[]{:S(2)}) async-start(f32[1,16,64,64]{3,2,1,0:T(8,128)} %copy-done.6), calls=%async_computation.8 | async-start | bytes 65536 | tf_op jit(solution)/shard_map/slice | solution.py:119
  472.1 11.1 %slice-start.1 = ((f32[1,32,64,64]{3,2,1,0:T(8,128)}), f32[1,1,64,64]{3,2,1,0:T(8,128)S(1)}, s32[]{:S(2)}) async-start(f32[1,32,64,64]{3,2,1,0:T(8,128)} %copy-done.7), calls=%async_computation.9 | async-start | bytes 65536 | tf_op jit(solution)/shard_map/slice | solution.py:119
  483.3 8.7 %copy-start.19 = (f32[32,64]{1,0:T(8,128)S(1)}, f32[32,64]{1,0:T(8,128)}, u32[]{:S(2)}) copy-start(f32[32,64]{1,0:T(8,128)} %copy-done.18) | copy-start | bytes 24580
  483.3 8.6 %copy-start.21 = (f32[32,128]{1,0:T(8,128)S(1)}, f32[32,128]{1,0:T(8,128)}, u32[]{:S(2)}) copy-start(f32[32,128]{1,0:T(8,128)} %copy-done.20) | copy-start | bytes 49156
  489.2 2.8 copy-start.17
  491.9 2.7 copy-start.3
  494.6 2.3 copy-start.5
  502.3 2.4 copy-start.23
  505.8 29.7 %all-to-all-start.5 = ((bf16[32,128,64]{1,2,0:T(8,128)(2,1)}), bf16[32,128,64]{1,2,0:T(8,128)(2,1)S(1)}, u32[]{:S(2)}, u32[]{:S(2)}) async-start(bf16[32,128,64]{1,2,0:T(8,128)(2,1)} %multiply_convert_fusion), calls=%async_computation.5 | async-start | bytes 1048576 | tf_op jit(solution)/shard_map/all_to_all | solution.py:164
  535.5 7.2 %copy-start.1 = (bf16[128,2048]{1,0:T(8,128)(2,1)S(1)}, bf16[128,2048]{1,0:T(8,128)(2,1)}, u32[]{:S(2)}) copy-start(bf16[128,2048]{1,0:T(8,128)(2,1)} %param.15) | copy-start | bytes 1572868
Sparse Core Ops, SparseCore 0:
  9.4 61.2 all-gather.4
  437.1 28.6 all-gather.6
